TPU v7x, 32 devices: a whole 2x2x4 slice. The times are simulated.
32 devices in a mesh: ep: 8 (over z, core), tp: 4 (over y, x).
Axes of the slice: x: 2, y: 2, z: 4, core: 2. Of those that a mesh axis runs over, the one named last changes fastest.
Arguments:
- branch_in: bfloat16 [8192, 512], P(('ep', 'tp')), may hold values from -6 to 6
- pool_weight: bfloat16 [4, 128, 128], replicated, may hold values from -0.5 to 0.5
- group_gain: float32 [512], replicated, may hold values from 0.1 to 1.9
- out_weight: bfloat16 [512, 2048], P(None, 'tp'), may hold values from -0.25 to 0.25
- out_gain: float32 [2048], replicated, may hold values from 0.1 to 1.9
- ffn_input: bfloat16 [1024, 2048], P('ep'), may hold values from -6 to 6
- ffn_gain: float32 [2048], replicated, may hold values from 0.1 to 1.9
- routes: int32 [1024, 4], P('ep'), may hold values from 0 to 7, all different within a row; in each aligned block of 128 rows (0 to 127, 128 to 255, ...) at most 128 rows name the same one
- route_weight: float32 [1024, 4], P('ep'), may hold values from 0.2 to 2
- gate_weight: bfloat16 [8, 2048, 4096], P('ep', None, 'tp'), may hold values from -0.375 to 0.375
- up_weight: bfloat16 [8, 2048, 4096], P('ep', None, 'tp'), may hold values from -0.375 to 0.375
- down_weight: bfloat16 [8, 4096, 2048], P('ep', 'tp'), may hold values from -0.0078125 to 0.0078125
Outputs:
- mixer_out: bfloat16 [8192, 2048], P(('ep', 'tp'))
- expert_out: bfloat16 [1024, 2048], P('ep', 'tp')
Inputs may be any that keep to these rules, and one draw needn't show every extreme that they name: `routes`: each row names 4 different experts. Among the 128 rows of one index of ep no expert is named by more than 128 rows, and in some such block one expert is named by exactly 128.
All inputs are finite; a program needn't handle non-finite values.
Results may differ from a plain program's by a relative error of at most 0.017.
Values may be sent and summed in bfloat16 or wider, within the bound.
A program may use at most 64 MiB of HBM per device.

v0:
```python
import jax
import jax.numpy as jnp
from jax import lax
from jax.sharding import PartitionSpec as P

pool_windows = (2, 4, 8, 16)
rim_rows = 15
norm_eps = 1e-06
clamp_limit = 7.0
sigmoid_slope = 1.702


def shifted_2(block, axis, distance):
    devices = range(lax.axis_size(axis))
    route = [(i - distance, i) for i in devices if i - distance in devices]
    return lax.ppermute(block, axis, route)


def rms_scale(values, gain):
    return values * lax.rsqrt(jnp.mean(values * values, axis=-1, keepdims=True) + norm_eps) * gain


def slot_tables(route_block, expert_count, capacity):
    row_count, top_count = route_block.shape
    flat_experts = route_block.reshape(-1)
    one_hot = (flat_experts[:, None] == jnp.arange(expert_count, dtype=jnp.int32)[None, :]).astype(
        jnp.int32
    )
    earlier = jnp.cumsum(one_hot, axis=0) - one_hot
    slot_index = jnp.sum(earlier * one_hot, axis=1)
    flat_slots = slot_index * expert_count + flat_experts
    owner_rows = jnp.full((capacity * expert_count,), row_count, jnp.int32)
    owner_rows = owner_rows.at[flat_slots].set(
        jnp.arange(row_count * top_count, dtype=jnp.int32) // top_count
    )
    return (flat_slots, owner_rows)


def pool_branch(branch_in, pool_weight, group_gain, out_weight, out_gain):
    row_count, width = branch_in.shape
    group_chans = width // len(pool_windows)
    rim = shifted_2(branch_in[row_count - rim_rows :], ("ep", "tp"), 1)
    widened = jnp.concatenate([rim, branch_in], axis=0).astype(jnp.float32)
    first_row = (lax.axis_index("ep") * lax.axis_size("tp") + lax.axis_index("tp")) * row_count
    positions = first_row + jnp.arange(row_count, dtype=jnp.int32)
    window = jnp.repeat(jnp.array(pool_windows, jnp.int32), group_chans)
    summed = jnp.zeros((row_count, width), jnp.float32)
    for offset_back in range(rim_rows + 1):
        shifted = widened[rim_rows - offset_back : rim_rows - offset_back + row_count]
        summed = summed + jnp.where(window[None, :] > offset_back, shifted, jnp.float32(0.0))
    counts = jnp.minimum(window[None, :], positions[:, None] + 1).astype(jnp.float32)
    pooled = (summed / counts - widened[rim_rows:]).astype(jnp.bfloat16)
    mixed_parts = []
    for group_index in range(len(pool_windows)):
        lower = group_index * group_chans
        mixed_parts.append(
            jnp.dot(
                pooled[:, lower : lower + group_chans],
                pool_weight[group_index],
                preferred_element_type=jnp.float32,
            )
        )
    group_mix = jnp.concatenate(mixed_parts, axis=1)
    mixed_rows = rms_scale(group_mix, group_gain).astype(jnp.bfloat16)
    projected = jnp.dot(
        mixed_rows,
        lax.all_gather(out_weight, "tp", axis=1, tiled=True),
        preferred_element_type=jnp.float32,
    )
    return rms_scale(projected, out_gain).astype(jnp.bfloat16)


def expert_hidden(slot_rows, gate_local, up_local):
    gate_pre = jnp.einsum("sed,df->sef", slot_rows, gate_local, preferred_element_type=jnp.float32)
    up_pre = jnp.einsum("sed,df->sef", slot_rows, up_local, preferred_element_type=jnp.float32)
    gate_pre = jnp.minimum(gate_pre, clamp_limit)
    up_pre = jnp.clip(up_pre, -clamp_limit, clamp_limit)
    return ((up_pre + 1.0) * gate_pre * jax.nn.sigmoid(sigmoid_slope * gate_pre)).astype(
        jnp.bfloat16
    )


def send_home(hidden, down_local):
    partial_sum = jnp.einsum("sef,fd->sed", hidden, down_local, preferred_element_type=jnp.float32)
    partial_sum = partial_sum.astype(jnp.bfloat16).astype(jnp.float32)
    summed = lax.psum_scatter(
        partial_sum.astype(jnp.bfloat16), "tp", scatter_dimension=2, tiled=True
    )
    return lax.all_to_all(summed, "ep", split_axis=1, concat_axis=1, tiled=True)


def per_device(
    branch_in,
    pool_weight,
    group_gain,
    out_weight,
    out_gain,
    ffn_input,
    ffn_gain,
    routes,
    route_weight,
    gate_weight,
    up_weight,
    down_weight,
):
    mixer_out = pool_branch(branch_in, pool_weight, group_gain, out_weight, out_gain)
    normed_rows = rms_scale(ffn_input.astype(jnp.float32), ffn_gain).astype(jnp.bfloat16)
    row_count, model_width = normed_rows.shape
    top_count = routes.shape[1]
    expert_count = lax.axis_size("ep")
    capacity = 2 * row_count * top_count // expert_count
    flat_slots, owner_rows = slot_tables(routes, expert_count, capacity)
    padded = jnp.concatenate([normed_rows, jnp.zeros((1, model_width), jnp.bfloat16)], axis=0)
    slot_rows = padded[owner_rows].reshape(capacity, expert_count, model_width)
    gate_local = gate_weight[0]
    up_local = up_weight[0]
    down_local = down_weight[0]
    share = capacity // lax.axis_size("tp")
    my_share = lax.dynamic_slice_in_dim(slot_rows, lax.axis_index("tp") * share, share, 0)
    arrived = lax.all_to_all(my_share, "ep", split_axis=1, concat_axis=1, tiled=True)
    hidden = expert_hidden(lax.all_gather(arrived, "tp", axis=0, tiled=True), gate_local, up_local)
    returned = send_home(hidden, down_local)
    column_count = returned.shape[2]
    picked = returned.reshape(capacity * expert_count, column_count)[flat_slots]
    picked = picked.reshape(row_count, top_count, column_count).astype(jnp.float32)
    expert_out = jnp.sum(picked * route_weight[:, :, None], axis=1).astype(jnp.bfloat16)
    return (mixer_out, expert_out)


def solution(mesh):
    in_specs = (
        P(("ep", "tp"), None),
        P(),
        P(),
        P(None, "tp"),
        P(),
        P("ep", None),
        P(),
        P("ep", None),
        P("ep", None),
        P("ep", None, "tp"),
        P("ep", None, "tp"),
        P("ep", "tp", None),
    )
    out_specs = (P(("ep", "tp"), None), P("ep", "tp"))
    return jax.shard_map(
        per_device, mesh=mesh, in_specs=in_specs, out_specs=out_specs, check_vma=False
    )
```

profile of v0, /device:TPU:0, one launch (start us, length us, event | category | flops | bytes accessed | tf_op | source)
XLA Modules:
  0.0 230.9 jit_solution(12385050998380482686)
XLA Ops:
  7.2 0.0 all-gather.5.cloned.1.call-start
  7.2 0.8 copy.16
  8.0 0.1 eq.29
  8.1 0.1 eq.25
  8.2 0.1 reshape.209
  8.4 1.1 reduce-window.6
  9.5 0.2 slice_reduce_fusion
  9.8 0.1 fusion.52
  9.9 2.4 %scatter_custom_fusion = s32[1024]{0:T(1024)S(1)} fusion(s32[512]{0:T(512)S(1)} %bitcast.66, s32[512]{0:T(512)S(1)} %add_select_fusion, s32[]{:T(128)} %constant.34.clone.1), kind=kCustom, calls=%fused_computation.109 | custom fusion | bytes 4100 | tf_op jit(solution)/shard_map/scatter | solution.py:33
  12.3 1.2 fusion.11
  13.6 1.2 fusion.13
  14.9 6.0 %gather_fusion = bf16[1024,2048]{1,0:T(8,128)(2,1)} fusion(bf16[129,2048]{1,0:T(8,128)(2,1)S(1)} %concatenate.11, s32[1024]{0:T(1024)S(1)} %fusion.54), kind=kCustom, calls=%fused_computation | custom fusion | bytes 8392704 | tf_op jit(solution)/shard_map/gather | solution.py:114
  20.9 1.3 constant_dynamic-slice_fusion
  22.2 0.6 copy.22
  22.8 32.8 %all_to_all.10 = bf16[32,8,2048]{2,0,1:T(8,128)(2,1)} all-to-all(bf16[32,8,2048]{2,0,1:T(8,128)(2,1)S(1)} %copy.22), channel_id=1, replica_groups=mesh['ep'=8,'tp'=4] {'ep'}, dimensions={1} | all-to-all | bytes 2097152 | tf_op jit(solution)/shard_map/all_to_all | solution.py:120
  55.6 0.0 all-gather.5.cloned.1.call-update
  55.6 0.0 reduce-scatter.2.cloned.1.call-start
  55.7 51.6 %all-gather.5.cloned.1.call-done = bf16[128,8,2048]{2,0,1:T(8,128)(2,1)} async-done(((bf16[32,8,2048]{2,0,1:T(8,128)(2,1)}), bf16[128,8,2048]{2,0,1:T(8,128)(2,1)}) %all-gather.5.cloned.1.call-update) | async-done | bytes 4194320 | tf_op jit(solution)/shard_map/all_gather | solution.py:121
  107.3 0.0 copy-start.6
  107.3 0.0 copy-start.8
  107.3 7.6 %fusion.2 = f32[128,8,1024]{2,0,1:T(8,128)S(1)} fusion(bf16[128,8,2048]{2,0,1:T(8,128)(2,1)} %all-gather.5.cloned.1.call-done, bf16[1,2048,1024]{2,1,0:T(8,128)(2,1)} %param.22), kind=kOutput, calls=%fused_computation.5 | convolution fusion | flops 4294967296 | bytes 12582912 | tf_op jit(solution)/shard_map/sed,df->sef/dot_general | solution.py:74
  114.9 0.0 copy-done.6
  115.0 0.0 copy-done.8
  115.0 0.0 copy-start.7
  115.0 5.7 %multiply_convert_fusion = bf16[128,8,1024]{2,0,1:T(8,128)(2,1)S(1)} fusion(f32[128,8,1024]{2,0,1:T(8,128)S(1)} %fusion.2, bf16[128,8,2048]{2,0,1:T(8,128)(2,1)S(1)} %copy-done.8, bf16[1,2048,1024]{2,1,0:T(8,128)(2,1)S(1)} %copy-done.6), kind=kOutput, calls=%fused_computation.9 | convolution fusion | flops 4305453056 | bytes 14680064 | tf_op jit(solution)/shard_map/sed,df->sef/dot_general | solution.py:75
  120.6 0.0 copy-done.7
  120.6 6.1 %fusion.6 = bf16[128,8,2048]{2,0,1:T(8,128)(2,1)} fusion(bf16[128,8,1024]{2,0,1:T(8,128)(2,1)S(1)} %multiply_convert_fusion, bf16[1,1024,2048]{2,1,0:T(8,128)(2,1)S(1)} %copy-done.7), kind=kOutput, calls=%fused_computation.10 | convolution fusion | flops 4297064448 | bytes 10485760 | tf_op jit(solution)/shard_map/sef,fd->sed/dot_general | solution.py:84
  126.7 0.0 copy-start
  126.7 0.0 copy-start.5
  126.7 0.0 copy-start.4
  126.7 0.0 reduce-scatter.2.cloned.1.call-update
  126.7 0.0 all-gather.3.cloned.1.call-start
  126.8 0.7 all-gather.3.cloned.1.call-update
  127.5 0.2 copy-done
  127.7 3.4 %collective-permute-start = (bf16[15,512]{1,0:T(8,128)(2,1)S(1)}, bf16[15,512]{1,0:T(8,128)(2,1)S(1)}, u32[]{:S(2)}, u32[]{:S(2)}) collective-permute-start(bf16[15,512]{1,0:T(8,128)(2,1)S(1)} %slice.82), channel_id=1, source_target_pairs={{0,1},{1,2},{2,3},{3,4},{4,5},{5,6},{6,7},{7,8},{8,9},{9,10},{10,1... | collective-permute-start | bytes 46088 | tf_op jit(solution)/shard_map/ppermute | solution.py:16
  131.1 0.0 copy-done.5
  131.1 0.1 broadcast_bitcast_fusion
  131.2 0.1 bitcast_compare_fusion.15
  131.3 0.0 copy-done.4
  131.3 0.1 copy.21
  131.4 1.1 collective-permute-done
  132.5 0.1 maximum_convert_fusion
  132.6 0.0 copy-start.1
  132.6 0.0 copy-start.3
  132.6 1.1 fusion.31
  133.7 0.0 copy-done.1
  133.7 0.0 copy-start.2
  133.8 0.2 fusion.35
  134.0 45.5 %reduce-scatter.2.cloned.1.call-done = bf16[128,8,512]{2,0,1:T(8,128)(2,1)} async-done(((bf16[128,8,2048]{2,0,1:T(8,128)(2,1)}), bf16[128,8,512]{2,0,1:T(8,128)(2,1)}) %reduce-scatter.2.cloned.1.call-update) | async-done | bytes 1048592 | tf_op jit(solution)/shard_map/reduce_scatter | solution.py:86
  179.5 4.6 %all-to-all-start.1 = ((bf16[128,8,512]{2,0,1:T(8,128)(2,1)}), bf16[128,8,512]{2,0,1:T(8,128)(2,1)S(1)}, u32[]{:S(2)}, u32[]{:S(2)}) async-start(bf16[128,8,512]{2,0,1:T(8,128)(2,1)} %reduce-scatter.2.cloned.1.call-done), calls=%async_computation.2 | async-start | bytes 2097152 | tf_op jit(solution)/shard_map/all_to_all | solution.py:89
  184.1 0.2 fusion.37
  184.3 0.2 fusion.39
  184.5 0.2 fusion.41
  184.8 0.1 multiply_reduce_fusion.2
  184.8 31.5 %all-gather.3.cloned.1.call-done = bf16[512,2048]{1,0:T(8,128)(2,1)} async-done(((bf16[512,512]{1,0:T(8,128)(2,1)}), bf16[512,2048]{1,0:T(8,128)(2,1)}) %all-gather.3.cloned.1.call-update) | async-done | bytes 2097168 | tf_op jit(solution)/shard_map/all_gather | solution.py:67
  216.4 0.0 copy-done.3
  216.4 2.5 %multiply_reduce_fusion = (f32[256]{0:T(256)S(1)}, f32[256,2048]{1,0:T(8,128)S(1)}) fusion(bf16[512,2048]{1,0:T(8,128)(2,1)} %all-gather.3.cloned.1.call-done, f32[256,128]{0,1:T(8,128)S(1)} %fusion.35, f32[256,128]{0,1:T(8,128)S(1)} %fusion.37, f32[256,128]{0,1:T(8,128)S(1)} %fusion.39, f32[256,128]{0,1:T(8,128)S(1)} %fusion.41, f32[512]{0:T(512)S(1)} %copy-done.3, ...), kind=kOutput, calls=%fused_computation.12 | convolution fusion | flops 538705664 | bytes 4722688 | tf_op jit(solution)/shard_map/dot_general | solution.py:65
  218.9 0.0 copy-done.2
  218.9 1.2 multiply_convert_fusion.1
  220.1 0.0 all-to-all-done.1
  220.2 0.6 copy.24
  220.7 2.0 gather_fusion.1
  222.7 0.3 reshape.212
  223.0 1.4 multiply_reduce_fusion.1
  (14 shorter events, 0.2 us)
Async XLA Ops:
  7.2 100.1 %all-gather.5.cloned.1.call-start = ((), (), s32[]{:S(2)}) async-start(), calls=%async_computation.4 | async-start | bytes 5242880 | tf_op jit(solution)/shard_map/all_gather | solution.py:121
  55.6 123.9 %reduce-scatter.2.cloned.1.call-start = ((), (), s32[]{:S(2)}) async-start(), calls=%async_computation.5 | async-start | bytes 5242880 | tf_op jit(solution)/shard_map/reduce_scatter | solution.py:86
  107.3 7.7 %copy-start.6 = (bf16[1,2048,1024]{2,1,0:T(8,128)(2,1)S(1)}, bf16[1,2048,1024]{2,1,0:T(8,128)(2,1)}, u32[]{:S(2)}) copy-start(bf16[1,2048,1024]{2,1,0:T(8,128)(2,1)} %param.23) | copy-start | bytes 12582916
  107.3 7.7 %copy-start.8 = (bf16[128,8,2048]{2,0,1:T(8,128)(2,1)S(1)}, bf16[128,8,2048]{2,0,1:T(8,128)(2,1)}, u32[]{:S(2)}) copy-start(bf16[128,8,2048]{2,0,1:T(8,128)(2,1)} %all-gather.5.cloned.1.call-done) | copy-start | bytes 12582916
  115.0 5.7 %copy-start.7 = (bf16[1,1024,2048]{2,1,0:T(8,128)(2,1)S(1)}, bf16[1,1024,2048]{2,1,0:T(8,128)(2,1)}, u32[]{:S(2)}) copy-start(bf16[1,1024,2048]{2,1,0:T(8,128)(2,1)} %param.24) | copy-start | bytes 12582916
  126.7 0.9 copy-start
  126.7 4.4 %copy-start.5 = (s32[4]{0:T(128)S(1)}, s32[4]{0:T(128)}, u32[]{:S(2)}) copy-start(s32[4]{0:T(128)} %constant.101.clone) | copy-start | bytes 52
  126.7 4.5 %copy-start.4 = (f32[128,4]{0,1:T(4,128)S(1)}, f32[128,4]{0,1:T(4,128)}, u32[]{:S(2)}) copy-start(f32[128,4]{0,1:T(4,128)} %param.21) | copy-start | bytes 6148
  126.7 89.6 %all-gather.3.cloned.1.call-start = ((), (), s32[]{:S(2)}) async-start(), calls=%async_computation.3 | async-start | bytes 2621440 | tf_op jit(solution)/shard_map/all_gather | solution.py:67
  127.7 4.8 %collective-permute-start = (bf16[15,512]{1,0:T(8,128)(2,1)S(1)}, bf16[15,512]{1,0:T(8,128)(2,1)S(1)}, u32[]{:S(2)}, u32[]{:S(2)}) collective-permute-start(bf16[15,512]{1,0:T(8,128)(2,1)S(1)} %slice.82), channel_id=1, source_target_pairs={{0,1},{1,2},{2,3},{3,4},{4,5},{5,6},{6,7},{7,8},{8,9},{9,10},{10,1... | collective-permute-start | bytes 46088 | tf_op jit(solution)/shard_map/ppermute | solution.py:16
  132.6 1.2 copy-start.1
  132.6 83.8 %copy-start.3 = (f32[512]{0:T(512)S(1)}, f32[512]{0:T(512)}, u32[]{:S(2)}) copy-start(f32[512]{0:T(512)} %param.15) | copy-start | bytes 6148
  133.7 85.2 %copy-start.2 = (f32[2048]{0:T(1024)S(1)}, f32[2048]{0:T(1024)}, u32[]{:S(2)}) copy-start(f32[2048]{0:T(1024)} %param.17) | copy-start | bytes 24580
  179.5 40.7 %all-to-all-start.1 = ((bf16[128,8,512]{2,0,1:T(8,128)(2,1)}), bf16[128,8,512]{2,0,1:T(8,128)(2,1)S(1)}, u32[]{:S(2)}, u32[]{:S(2)}) async-start(bf16[128,8,512]{2,0,1:T(8,128)(2,1)} %reduce-scatter.2.cloned.1.call-done), calls=%async_computation.2 | async-start | bytes 2097152 | tf_op jit(solution)/shard_map/all_to_all | solution.py:89
Sparse Core Ops, SparseCore 0:
  55.7 51.4 all-gather.4
  126.9 52.5 reduce-scatter.1
  181.3 35.0 all-gather.2
where the time goes:
time: 231 us
  waiting for transfers between devices  130 us (56%)
  blocking collectives  32.8 us (14%)
  matrix products  22.7 us (10%)
  local copies, waits for them, and re-layouts  15 us (6%)
  between operations  14 us (6%)
  starting transfers between devices  8.11 us (4%)
  other arithmetic  7.78 us (3%)
    all_gather x1, waiting for transfers between devices, per_device(): lax.all_gather(arrived, 'tp', axis=0, tiled=True)  51.6 us
    reduce_scatter x1, waiting for transfers between devices, send_home(): lax.psum_scatter(partial_sum.astype(jnp.bfloat16), 'tp', scatter_dimensio...  45.5 us
    all_to_all x1, blocking collectives, per_device(): lax.all_to_all(my_share, 'ep', split_axis=1, concat_axis=1, tiled=True)  32.8 us
    all_gather x1, waiting for transfers between devices, pool_branch(): lax.all_gather(out_weight, 'tp', axis=1, tiled=True)  31.5 us
    dot_general x1, matrix products, expert_hidden(): jnp.einsum('sed,df->sef', slot_rows, gate_local, preferred_element_type=j...  7.64 us
    dot_general x1, matrix products, send_home(): jnp.einsum('sef,fd->sed', hidden, down_local, preferred_element_type=jnp....  6.07 us
    gather x1, local copies, waits for them, and re-layouts, per_device(): slot_rows = padded[owner_rows].reshape(capacity, expert_count, model_width)  6.02 us
    dot_general x1, matrix products, expert_hidden(): jnp.einsum('sed,df->sef', slot_rows, up_local, preferred_element_type=jnp...  5.65 us
  transfers between devices with their start and end apart: 5, of which 4 were waited for; matrix products, arithmetic and copies ran while one was open for 3% of the time, Pallas kernels for 0%

commit v1 on v0

--- a/solution.py
+++ b/solution.py
@@ -8,6 +8,18 @@
 norm_eps = 1e-06
 clamp_limit = 7.0
 sigmoid_slope = 1.702
+
+
+def gather_by_bits(value, axis, dim):
+    ways, here = (lax.axis_size(axis), lax.axis_index(axis))
+    grown, reach = (value, 1)
+    while reach < ways:
+        theirs = lax.ppermute(grown, axis, [(d, d ^ reach) for d in range(ways)])
+        mine_first = jnp.concatenate([grown, theirs], axis=dim)
+        theirs_first = jnp.concatenate([theirs, grown], axis=dim)
+        grown = jnp.where(here & reach == 0, mine_first, theirs_first)
+        reach = 2 * reach
+    return grown
 
 
 def shifted_2(block, axis, distance):
@@ -118,7 +130,7 @@
     share = capacity // lax.axis_size("tp")
     my_share = lax.dynamic_slice_in_dim(slot_rows, lax.axis_index("tp") * share, share, 0)
     arrived = lax.all_to_all(my_share, "ep", split_axis=1, concat_axis=1, tiled=True)
-    hidden = expert_hidden(lax.all_gather(arrived, "tp", axis=0, tiled=True), gate_local, up_local)
+    hidden = expert_hidden(gather_by_bits(arrived, "tp", 0), gate_local, up_local)
     returned = send_home(hidden, down_local)
     column_count = returned.shape[2]
     picked = returned.reshape(capacity * expert_count, column_count)[flat_slots]

time: 231 us -> 260 us (1.13)
  waiting for transfers between devices: 130 us -> 147 us
  matrix products: 22.7 us -> 29.7 us
  starting transfers between devices: 8.11 us -> 11.3 us
    ppermute x0 -> x2, waiting for transfers between devices: none -> 67.9 us  [gather_by_bits(): theirs = lax.ppermute(grown, axis, [(d, d ^ reach) for d in range(ways)])]
    all_gather x1 -> x0, waiting for transfers between devices: 51.6 us -> none  [per_device(): lax.all_gather(arrived, 'tp', axis=0, tiled=True)]
    dot_general x1, matrix products: 6.07 us -> 16.5 us  [send_home(): jnp.einsum('sef,fd->sed', hidden, down_local, preferred_element_type=jnp....]
    dot_general x1 -> x0, matrix products: 7.64 us -> none  [expert_hidden(): jnp.einsum('sed,df->sef', slot_rows, gate_local, preferred_element_type=j...]
    dot_general x1, matrix products: 5.65 us -> 9.94 us  [expert_hidden(): jnp.einsum('sed,df->sef', slot_rows, up_local, preferred_element_type=jnp...]
    ppermute x0 -> x2, starting transfers between devices: none -> 3.08 us  [gather_by_bits(): theirs = lax.ppermute(grown, axis, [(d, d ^ reach) for d in range(ways)])]
  transfers between devices with their start and end apart: 5 -> 6, of which waited for: 4 -> 5; matrix products, arithmetic and copies ran while one was open for 3% -> 2% of each run, Pallas kernels for 0% -> 0%
where the time goes in v1:
time: 260 us
  waiting for transfers between devices  147 us (57%)
  blocking collectives  32.7 us (13%)
  matrix products  29.7 us (11%)
  local copies, waits for them, and re-layouts  15 us (6%)
  between operations  14.3 us (6%)
  starting transfers between devices  11.3 us (4%)
  other arithmetic  10.2 us (4%)
    ppermute x2, waiting for transfers between devices, gather_by_bits(): theirs = lax.ppermute(grown, axis, [(d, d ^ reach) for d in range(ways)])  67.9 us
    reduce_scatter x1, waiting for transfers between devices, send_home(): lax.psum_scatter(partial_sum.astype(jnp.bfloat16), 'tp', scatter_dimensio...  45.7 us
    all_to_all x1, blocking collectives, per_device(): lax.all_to_all(my_share, 'ep', split_axis=1, concat_axis=1, tiled=True)  32.7 us
    all_gather x1, waiting for transfers between devices, pool_branch(): lax.all_gather(out_weight, 'tp', axis=1, tiled=True)  31.6 us
    dot_general x1, matrix products, send_home(): jnp.einsum('sef,fd->sed', hidden, down_local, preferred_element_type=jnp....  16.5 us
    dot_general x1, matrix products, expert_hidden(): jnp.einsum('sed,df->sef', slot_rows, up_local, preferred_element_type=jnp...  9.94 us
    gather x1, local copies, waits for them, and re-layouts, per_device(): slot_rows = padded[owner_rows].reshape(capacity, expert_count, model_width)  6.02 us
  transfers between devices with their start and end apart: 6, of which 5 were waited for; matrix products, arithmetic and copies ran while one was open for 2% of the time, Pallas kernels for 0%

profile of v1, /device:TPU:0, one launch (start us, length us, event | category | flops | bytes accessed | tf_op | source)
XLA Modules:
  0.0 259.9 jit_solution(3403495987471954472)
XLA Ops:
  7.2 0.0 reduce-scatter.2.cloned.1.call-start
  7.2 0.8 copy.17
  8.0 0.1 eq.37
  8.1 0.1 eq.33
  8.2 0.1 reshape.209
  8.4 1.1 reduce-window.6
  9.5 0.2 slice_reduce_fusion
  9.8 0.1 fusion.54
  9.9 2.4 scatter_custom_fusion
  12.3 1.2 fusion.11
  13.6 1.2 fusion.13
  14.9 6.0 %gather_fusion = bf16[1024,2048]{1,0:T(8,128)(2,1)} fusion(bf16[129,2048]{1,0:T(8,128)(2,1)S(1)} %concatenate.23, s32[1024]{0:T(1024)S(1)} %fusion.56), kind=kCustom, calls=%fused_computation | custom fusion | bytes 8392704 | tf_op jit(solution)/shard_map/gather | solution.py:126
  20.9 1.3 constant_dynamic-slice_fusion
  22.2 0.6 copy.23
  22.8 32.7 %all_to_all.10 = bf16[32,8,2048]{2,0,1:T(8,128)(2,1)S(1)} all-to-all(bf16[32,8,2048]{2,0,1:T(8,128)(2,1)S(1)} %copy.23), channel_id=1, replica_groups=mesh['ep'=8,'tp'=4] {'ep'}, dimensions={1} | all-to-all | bytes 2097152 | tf_op jit(solution)/shard_map/all_to_all | solution.py:132
  55.5 1.5 collective-permute-start.1
  57.0 23.1 %collective-permute-done.1 = bf16[32,8,2048]{2,0,1:T(8,128)(2,1)} collective-permute-done((bf16[32,8,2048]{2,0,1:T(8,128)(2,1)S(1)}, bf16[32,8,2048]{2,0,1:T(8,128)(2,1)}, u32[]{:S(2)}, u32[]{:S(2)}) %collective-permute-start.1) | collective-permute-done | bytes 1048608 | tf_op jit(solution)/shard_map/ppermute | solution.py:17
  80.1 2.4 maximum_select_fusion.1
  82.5 1.6 collective-permute-start.2
  84.1 44.7 %collective-permute-done.2 = bf16[64,8,2048]{2,0,1:T(8,128)(2,1)} collective-permute-done((bf16[64,8,2048]{2,0,1:T(8,128)(2,1)S(1)}, bf16[64,8,2048]{2,0,1:T(8,128)(2,1)}, u32[]{:S(2)}, u32[]{:S(2)}) %collective-permute-start.2) | collective-permute-done | bytes 2097184 | tf_op jit(solution)/shard_map/ppermute | solution.py:17
  128.8 9.9 %fusion.4 = f32[128,8,1024]{2,0,1:T(8,128)} fusion(bf16[1,2048,1024]{2,1,0:T(8,128)(2,1)} %param.23, bf16[64,8,2048]{2,0,1:T(8,128)(2,1)} %collective-permute-done.2, bf16[64,8,2048]{2,0,1:T(8,128)(2,1)S(1)} %maximum_select_fusion.1, pred[]{:T(512)S(6)} %eq.31), kind=kOutput, calls=%fused_computation.8 | convolution fusion | flops 4313841664 | bytes 12582913 | tf_op jit(solution)/shard_map/sed,df->sef/dot_general | solution.py:87
  138.8 16.5 %fusion.6 = bf16[128,8,2048]{2,0,1:T(8,128)(2,1)} fusion(bf16[1,1024,2048]{2,1,0:T(8,128)(2,1)} %param.24, f32[128,8,1024]{2,0,1:T(8,128)} %fusion.4, bf16[1,2048,1024]{2,1,0:T(8,128)(2,1)} %param.22, bf16[64,8,2048]{2,0,1:T(8,128)(2,1)} %collective-permute-done.2, bf16[64,8,2048]{2,0,1:T(8,128)(2,1)S(1)} %maximum_select_fusion.1, pred[]{:T(512)S(6)} %eq.31), kind=kOutput, calls=%fused_computation.11 | convolution fusion | flops 8621391872 | bytes 20971520 | tf_op jit(solution)/shard_map/sef,fd->sed/dot_general | solution.py:96
  155.2 0.0 copy-start
  155.2 0.0 copy-start.5
  155.2 0.0 copy-start.4
  155.3 0.0 reduce-scatter.2.cloned.1.call-update
  155.3 0.0 all-gather.2.cloned.1.call-start
  155.3 0.7 all-gather.2.cloned.1.call-update
  156.0 0.2 copy-done
  156.2 3.6 %collective-permute-start = (bf16[15,512]{1,0:T(8,128)(2,1)S(1)}, bf16[15,512]{1,0:T(8,128)(2,1)S(1)}, u32[]{:S(2)}, u32[]{:S(2)}) collective-permute-start(bf16[15,512]{1,0:T(8,128)(2,1)S(1)} %slice.82), channel_id=1, source_target_pairs={{0,1},{1,2},{2,3},{3,4},{4,5},{5,6},{6,7},{7,8},{8,9},{9,10},{10,1... | collective-permute-start | bytes 46088 | tf_op jit(solution)/shard_map/ppermute | solution.py:28
  159.8 0.0 copy-done.5
  159.8 0.1 broadcast_bitcast_fusion
  159.9 0.1 bitcast_compare_fusion.15
  160.0 0.0 copy-done.4
  160.0 0.1 copy.22
  160.1 0.9 collective-permute-done
  161.0 0.1 maximum_convert_fusion
  161.1 0.0 copy-start.1
  161.1 0.0 copy-start.3
  161.1 1.1 fusion.33
  162.3 0.0 copy-done.1
  162.3 0.0 copy-start.2
  162.3 0.2 fusion.37
  162.5 45.7 %reduce-scatter.2.cloned.1.call-done = bf16[128,8,512]{2,0,1:T(8,128)(2,1)} async-done(((bf16[128,8,2048]{2,0,1:T(8,128)(2,1)}), bf16[128,8,512]{2,0,1:T(8,128)(2,1)}) %reduce-scatter.2.cloned.1.call-update) | async-done | bytes 1048592 | tf_op jit(solution)/shard_map/reduce_scatter | solution.py:98
  208.2 4.6 %all-to-all-start.1 = ((bf16[128,8,512]{2,0,1:T(8,128)(2,1)}), bf16[128,8,512]{2,0,1:T(8,128)(2,1)S(1)}, u32[]{:S(2)}, u32[]{:S(2)}) async-start(bf16[128,8,512]{2,0,1:T(8,128)(2,1)} %reduce-scatter.2.cloned.1.call-done), calls=%async_computation.2 | async-start | bytes 2097152 | tf_op jit(solution)/shard_map/all_to_all | solution.py:101
  212.8 0.2 fusion.39
  213.0 0.2 fusion.41
  213.2 0.2 fusion.43
  213.4 0.1 multiply_reduce_fusion.2
  213.5 31.6 %all-gather.2.cloned.1.call-done = bf16[512,2048]{1,0:T(8,128)(2,1)} async-done(((bf16[512,512]{1,0:T(8,128)(2,1)}), bf16[512,2048]{1,0:T(8,128)(2,1)}) %all-gather.2.cloned.1.call-update) | async-done | bytes 2097168 | tf_op jit(solution)/shard_map/all_gather | solution.py:79
  245.1 0.0 copy-done.3
  245.1 2.5 multiply_reduce_fusion
  247.6 0.0 copy-done.2
  247.6 1.2 multiply_convert_fusion.1
  248.8 0.0 all-to-all-done.1
  248.8 0.6 copy.25
  249.4 2.0 gather_fusion.1
  251.4 0.3 reshape.212
  251.7 1.4 multiply_reduce_fusion.1
  (14 shorter events, 0.2 us)
Async XLA Ops:
  7.2 201.0 %reduce-scatter.2.cloned.1.call-start = ((), (), s32[]{:S(2)}) async-start(), calls=%async_computation.4 | async-start | bytes 5242880 | tf_op jit(solution)/shard_map/reduce_scatter | solution.py:98
  55.5 24.6 %collective-permute-start.1 = (bf16[32,8,2048]{2,0,1:T(8,128)(2,1)S(1)}, bf16[32,8,2048]{2,0,1:T(8,128)(2,1)}, u32[]{:S(2)}, u32[]{:S(2)}) collective-permute-start(bf16[32,8,2048]{2,0,1:T(8,128)(2,1)S(1)} %all_to_all.10), channel_id=1, source_target_pairs={{0,1},{1,0},{2,3},{3,2},{4,5},{5,4},{6,7},{7,6},{8,9},{9,8},{10,11... | collective-permute-start | bytes 3145736 | tf_op jit(solution)/shard_map/ppermute | solution.py:17
  82.5 46.3 %collective-permute-start.2 = (bf16[64,8,2048]{2,0,1:T(8,128)(2,1)S(1)}, bf16[64,8,2048]{2,0,1:T(8,128)(2,1)}, u32[]{:S(2)}, u32[]{:S(2)}) collective-permute-start(bf16[64,8,2048]{2,0,1:T(8,128)(2,1)S(1)} %maximum_select_fusion.1), channel_id=1, source_target_pairs={{0,2},{1,3},{2,0},{3,1},{4,6},{5,7},{6,4},{7,5},{8,10},{9,11},{10,... | collective-permute-start | bytes 6291464 | tf_op jit(solution)/shard_map/ppermute | solution.py:17
  155.2 0.9 copy-start
  155.2 4.6 %copy-start.5 = (s32[4]{0:T(128)S(1)}, s32[4]{0:T(128)}, u32[]{:S(2)}) copy-start(s32[4]{0:T(128)} %constant.103.clone) | copy-start | bytes 52
  155.2 4.7 %copy-start.4 = (f32[128,4]{0,1:T(4,128)S(1)}, f32[128,4]{0,1:T(4,128)}, u32[]{:S(2)}) copy-start(f32[128,4]{0,1:T(4,128)} %param.21) | copy-start | bytes 6148
  155.3 89.8 %all-gather.2.cloned.1.call-start = ((), (), s32[]{:S(2)}) async-start(), calls=%async_computation.3 | async-start | bytes 2621440 | tf_op jit(solution)/shard_map/all_gather | solution.py:79
  156.2 4.8 %collective-permute-start = (bf16[15,512]{1,0:T(8,128)(2,1)S(1)}, bf16[15,512]{1,0:T(8,128)(2,1)S(1)}, u32[]{:S(2)}, u32[]{:S(2)}) collective-permute-start(bf16[15,512]{1,0:T(8,128)(2,1)S(1)} %slice.82), channel_id=1, source_target_pairs={{0,1},{1,2},{2,3},{3,4},{4,5},{5,6},{6,7},{7,8},{8,9},{9,10},{10,1... | collective-permute-start | bytes 46088 | tf_op jit(solution)/shard_map/ppermute | solution.py:28
  161.1 1.2 copy-start.1
  161.1 84.0 %copy-start.3 = (f32[512]{0:T(512)S(1)}, f32[512]{0:T(512)}, u32[]{:S(2)}) copy-start(f32[512]{0:T(512)} %param.15) | copy-start | bytes 6148
  162.3 85.3 %copy-start.2 = (f32[2048]{0:T(1024)S(1)}, f32[2048]{0:T(1024)}, u32[]{:S(2)}) copy-start(f32[2048]{0:T(1024)} %param.17) | copy-start | bytes 24580
  208.2 40.6 %all-to-all-start.1 = ((bf16[128,8,512]{2,0,1:T(8,128)(2,1)}), bf16[128,8,512]{2,0,1:T(8,128)(2,1)S(1)}, u32[]{:S(2)}, u32[]{:S(2)}) async-start(bf16[128,8,512]{2,0,1:T(8,128)(2,1)} %reduce-scatter.2.cloned.1.call-done), calls=%async_computation.2 | async-start | bytes 2097152 | tf_op jit(solution)/shard_map/all_to_all | solution.py:101
Sparse Core Ops, SparseCore 0:
  155.4 52.7 reduce-scatter.1
  210.0 35.0 all-gather.1
